TPU v7x, 32 devices: a whole 2x2x4 slice. The times are simulated.
32 devices in a mesh: ep: 8 (over z, x), tp: 4 (over y, core).
Axes of the slice: x: 2, y: 2, z: 4, core: 2. Of those that a mesh axis runs over, the one named last changes fastest.
Arguments:
- queries: bfloat16 [1024, 4096], P('ep', 'tp'), may hold values from -112 to 112
- key_rows: bfloat16 [1024, 4096], P('ep', 'tp'), may hold values from -8.1 to 8.1
- values: bfloat16 [1024, 4096], P('ep', 'tp'), may hold values from -6 to 6
- lambdas: float32 [16], P('tp'), may hold values from 0.3 to 0.8
- head_gain: float32 [256], replicated, may hold values from 0.1 to 1.9
- tokens: bfloat16 [512, 4096], P('ep'), may hold values from -6 to 6
- moe_gain: float32 [4096], replicated, may hold values from 0.1 to 1.9
- routes: int32 [512, 2], P('ep'), may hold values from 0 to 7, all different within a row; in each aligned block of 64 rows (0 to 63, 64 to 127, ...) at most 32 rows name the same one
- route_scores: float32 [512, 2], P('ep'), may hold values from -6 to 6
- w_gate: bfloat16 [8, 4096, 2048], P('ep', None, 'tp'), may hold values from -0.09375 to 0.09375
- w_up: bfloat16 [8, 4096, 2048], P('ep', None, 'tp'), may hold values from -0.09375 to 0.09375
- w_down: bfloat16 [8, 2048, 4096], P('ep', 'tp'), may hold values from -0.125 to 0.125
Outputs:
- attended: bfloat16 [1024, 4096], P('ep', 'tp')
- expert_out: bfloat16 [512, 4096], P('ep', 'tp')
Inputs may be any that keep to these rules, and one draw needn't show every extreme that they name: `routes`: each row names 2 different experts. Among the rows of one index of ep at most 32 name the same expert, and some index reaches 32 in every draw.
All inputs are finite; a program needn't handle non-finite values.
Results may differ from a plain program's by a relative error of at most 0.018.
Values may be sent and summed in bfloat16 or wider, within the bound.
A program may use at most 64 MiB of HBM per device.

v0:
```python
import functools

import jax
import jax.numpy as jnp
from jax import lax
from jax.experimental import pallas as pl
from jax.experimental.pallas import tpu as pltpu
from jax.sharding import PartitionSpec as P

QKD = 128
VD = 256
TOP = 2


neg_big = -1e30
head_eps = 1e-05
moe_eps = 1e-06
head_scale = 0.8


def slot_table(routes, experts, capacity):
    flat_routes = routes.reshape(-1)
    onehot = (flat_routes[:, None] == jnp.arange(experts, dtype=jnp.int32)[None, :]).astype(
        jnp.int32
    )
    before = jnp.cumsum(onehot, axis=0) - onehot
    position = jnp.sum(before * onehot, axis=1)
    return (flat_routes * capacity + position).reshape(routes.shape)


def fold_block(state, query_group, query_pos, key_heads, value_heads, key_pos):
    maxima, denominators, accumulated = state
    scores = jnp.einsum(
        "qhmd,khmd->hmqk", query_group, key_heads, preferred_element_type=jnp.float32
    ) * QKD ** (-0.5)
    visible = key_pos[None, :] <= query_pos[:, None]
    scores = jnp.where(visible, scores, neg_big)
    new_max = jnp.maximum(maxima, jnp.max(scores, axis=-1))
    weights = jnp.where(visible, jnp.exp(scores - new_max[..., None]), 0.0)
    accumulated = jnp.einsum(
        "hmqk,khd->hmqd", weights, value_heads, precision=lax.Precision.HIGHEST
    )
    denominators = jnp.sum(weights, axis=-1)
    return (new_max, denominators, accumulated)


def local_general(
    queries,
    key_rows,
    values,
    lambdas,
    head_gain,
    tokens,
    moe_gain,
    routes,
    route_scores,
    w_gate,
    w_up,
    w_down,
):
    rows_a = queries.shape[0]
    half_rows = rows_a // 2
    head_local = lambdas.shape[0]
    ep_count = lax.axis_size("ep")
    ep_index = lax.axis_index("ep")
    early_queries = queries[:half_rows]
    later_queries = queries[half_rows:]
    early_pos = ep_index * rows_a + jnp.arange(half_rows, dtype=jnp.int32)
    later_pos = ep_index * rows_a + half_rows + jnp.arange(half_rows, dtype=jnp.int32)
    query_groups = (
        early_queries.reshape(half_rows, head_local, 2, QKD),
        later_queries.reshape(half_rows, head_local, 2, QKD),
    )
    position_groups = (early_pos, later_pos)
    start_state = (
        jnp.full((head_local, 2, half_rows), neg_big, jnp.float32),
        jnp.zeros((head_local, 2, half_rows), jnp.float32),
        jnp.zeros((head_local, 2, half_rows, VD), jnp.float32),
    )
    totals = (start_state, start_state)
    row_start = jnp.int32(0)
    key_block = lax.all_gather(key_rows, "ep", axis=0, tiled=True)
    value_block = lax.all_gather(values, "ep", axis=0, tiled=True)
    key_count = key_block.shape[0]
    key_heads = key_block.reshape(key_count, head_local, 2, QKD)
    value_heads = value_block.reshape(key_count, head_local, VD).astype(jnp.float32)
    key_pos = jnp.arange(key_count, dtype=jnp.int32)
    updated = []
    for attend_group_index in range(2):
        state = totals[attend_group_index]
        query_group = query_groups[attend_group_index]
        query_pos = position_groups[attend_group_index]
        state = lax.cond(
            row_start <= query_pos[-1],
            lambda held: fold_block(held, query_group, query_pos, key_heads, value_heads, key_pos),
            lambda held: held,
            state,
        )
        updated.append(state)
    folded = (updated[0], updated[1])
    attended_groups = []
    for group_index in range(2):
        maxima, denominators, accumulated = folded[group_index]
        mixed_out = (
            accumulated[:, 0] / denominators[:, 0, :, None]
            - lambdas[:, None, None] * accumulated[:, 1] / denominators[:, 1, :, None]
        )
        scaled = mixed_out * lax.rsqrt(
            jnp.mean(mixed_out * mixed_out, axis=-1, keepdims=True) + head_eps
        )
        scaled = scaled * head_gain * head_scale
        attended_groups.append(
            scaled.transpose(1, 0, 2).reshape(half_rows, head_local * VD).astype(jnp.bfloat16)
        )
    later_out = attended_groups[1]
    attended = jnp.concatenate([attended_groups[0], later_out], axis=0)
    rows_b = tokens.shape[0]
    capacity = 2 * TOP * rows_b // ep_count
    token_f32 = tokens.astype(jnp.float32)
    normed = (
        token_f32
        * lax.rsqrt(jnp.mean(token_f32 * token_f32, axis=-1, keepdims=True) + moe_eps)
        * moe_gain
    ).astype(jnp.bfloat16)
    gate_weights = jax.nn.softmax(route_scores, axis=-1)
    slot_of = slot_table(routes, ep_count, capacity)
    row_ids = jnp.broadcast_to(jnp.arange(rows_b, dtype=jnp.int32)[:, None], slot_of.shape)
    row_of_slot = (
        jnp.zeros((ep_count * capacity,), jnp.int32)
        .at[slot_of.reshape(-1)]
        .set(row_ids.reshape(-1))
    )
    gate_local = w_gate[0]
    up_local = w_up[0]
    down_local = w_down[0]
    outgoing = normed[row_of_slot]
    arrived = lax.all_to_all(outgoing, "ep", split_axis=0, concat_axis=0, tiled=True)
    gate_act = jnp.dot(arrived, gate_local, preferred_element_type=jnp.float32)
    up_act = jnp.dot(arrived, up_local, preferred_element_type=jnp.float32)
    hidden = (jax.nn.silu(gate_act) * up_act).astype(jnp.bfloat16)
    summed = lax.psum_scatter(
        lax.dot_general(
            down_local, hidden, (((0,), (1,)), ((), ())), preferred_element_type=jnp.float32
        ).astype(jnp.bfloat16),
        "tp",
        scatter_dimension=0,
        tiled=True,
    )
    returned = lax.all_to_all(summed, "ep", split_axis=1, concat_axis=1, tiled=True)
    slot_ids = jnp.arange(ep_count * capacity, dtype=jnp.int32)
    combined = jnp.zeros((rows_b, returned.shape[0]), jnp.float32)
    for choice_index in range(TOP):
        picker = (slot_of[:, choice_index, None] == slot_ids[None, :]).astype(jnp.bfloat16)
        picked = lax.dot_general(
            picker, returned, (((1,), (1,)), ((), ())), preferred_element_type=jnp.float32
        )
        combined = combined + gate_weights[:, choice_index, None] * picked
    expert_out = combined.astype(jnp.bfloat16)
    return (attended, expert_out)


MESH = pl.DeviceIdType.MESH


def step_kernel(
    n,
    heads,
    q_ref,
    k_ref,
    v_ref,
    lam_ref,
    gain_ref,
    tokens_ref,
    moe_gain_ref,
    routes_ref,
    score_ref,
    wg_ref,
    wu_ref,
    wd_ref,
    att_ref,
    out_ref,
    wg,
    wu,
    wd,
    qbuf,
    kbuf,
    vbuf,
    osend,
    oret,
    fin,
    att_in,
    pick,
    tok,
    arr,
    part,
    near,
    csum,
    far,
    res,
    ret,
    w_sem,
    tok_send,
    tok_recv,
    ty_send,
    ty_recv,
    tc_send,
    tc_recv,
    a_send,
    a_recv,
    v_send,
    v_recv,
    o_send,
    o_recv,
    f_send,
    f_recv,
    rc_send,
    rc_recv,
    ry_send,
    ry_recv,
    e_send,
    e_recv,
):
    me = lax.axis_index("ep")
    tp = lax.axis_index("tp")
    y = tp // 2
    core = tp % 2
    tp_core = y * 2 + 1 - core
    tp_y = (1 - y) * 2 + core
    tp_both = (1 - y) * 2 + 1 - core
    side = me % 2
    head = me // 2
    pair = head * 2 + 1 - side
    rows = q_ref.shape[0]
    rows_b = tokens_ref.shape[0]
    _, slots, width = tok.shape
    total = n * slots

    def peer(j):
        return lax.rem(me + j, n)

    def source(j):
        return lax.rem(me + n - j, n)

    def remote(src, dst, send, recv, ep, tpi):
        return pltpu.make_async_remote_copy(
            src_ref=src,
            dst_ref=dst,
            send_sem=send,
            recv_sem=recv,
            device_id=(ep, tpi),
            device_id_type=MESH,
        )

    barrier = pltpu.get_barrier_semaphore()
    for j in range(1, n):
        pl.semaphore_signal(barrier, inc=1, device_id=(peer(j), tp), device_id_type=MESH)
    pl.semaphore_signal(barrier, inc=1, device_id=(me, tp_core), device_id_type=MESH)
    pl.semaphore_signal(barrier, inc=1, device_id=(me, tp_y), device_id_type=MESH)
    loads = [
        pltpu.make_async_copy(wg_ref.at[0], wg, w_sem.at[0]),
        pltpu.make_async_copy(wu_ref.at[0], wu, w_sem.at[1]),
        pltpu.make_async_copy(wd_ref.at[0], wd, w_sem.at[2]),
    ]
    for load in loads:
        load.start()

    features = pl.ds(pl.multiple_of(tp * width, width), width)
    token_f32 = tokens_ref[...].astype(jnp.float32)
    inverse = lax.rsqrt(jnp.mean(token_f32 * token_f32, axis=-1, keepdims=True) + moe_eps)
    normed = (
        tokens_ref[:, features].astype(jnp.float32) * inverse * moe_gain_ref[:, features]
    ).astype(jnp.bfloat16)
    lane = lax.broadcasted_iota(jnp.int32, (rows_b, 128), 1)
    square = (rows_b, rows_b)
    row_at = lax.broadcasted_iota(jnp.int32, square, 0)
    column_at = lax.broadcasted_iota(jnp.int32, square, 1)

    def upright(ref, c):
        line = jnp.broadcast_to(ref[c : c + 1, :], square)
        return jnp.sum(
            jnp.where(row_at == column_at, line, jnp.zeros_like(line)), axis=1, keepdims=True
        )

    named_by = [upright(routes_ref, c) for c in range(TOP)]
    named = [named_by[c] == lane for c in range(TOP)]
    either = jnp.where(named[0] | named[1], 1.0, 0.0).astype(jnp.bfloat16)
    below = jnp.where(column_at < row_at, 1.0, 0.0).astype(jnp.bfloat16)
    before = jnp.dot(below, either, preferred_element_type=jnp.float32)
    slot_ids = lax.broadcasted_iota(jnp.int32, (rows_b, total), 1).astype(jnp.float32)
    chosen = jnp.zeros((rows_b, total), jnp.float32)
    for c in range(TOP):
        position = jnp.sum(jnp.where(named[c], before, 0.0), axis=1, keepdims=True)
        slot = named_by[c].astype(jnp.float32) * slots + position
        hit = jnp.where(slot == slot_ids, 1.0, 0.0)
        pick[c] = hit.astype(jnp.bfloat16)
        chosen = chosen + hit
    tok[...] = (
        jnp.dot(chosen.T.astype(jnp.bfloat16), normed, preferred_element_type=jnp.float32)
        .astype(jnp.bfloat16)
        .reshape(n, slots, width)
    )
    pl.semaphore_wait(barrier, n + 1)

    sent = []
    tok_copies = []
    for j in range(1, n):
        c = remote(tok.at[peer(j)], arr.at[tp, me], tok_send.at[j], tok_recv.at[j], peer(j), tp)
        c.start()
        tok_copies.append(c)
    unit_copies = {}
    for which, src, dst in ((0, v_ref, None), (1, k_ref, kbuf.at[me]), (2, q_ref, qbuf.at[me])):
        for j in range(1, n):
            d = peer(j)
            cols = pl.ds(pl.multiple_of(d * QKD, QKD), QKD)
            to = vbuf.at[d % 2, me] if which == 0 else dst
            c = remote(src.at[:, cols], to, a_send.at[which, j], a_recv.at[which, j], d, tp)
            c.start()
            unit_copies[which, j] = c
    own = pl.ds(pl.multiple_of(me * QKD, QKD), QKD)
    qbuf[me] = q_ref[:, own]
    kbuf[me] = k_ref[:, own]
    vbuf[side, me] = v_ref[:, own]
    v_copies = [
        remote(v_ref.at[:, own], vbuf.at[side, me], v_send.at[me], v_recv.at[me], pair, tp)
    ]
    v_copies[0].start()

    y_copies, core_copies = [], ([], [])
    for j in range(n):
        s = source(j)
        if j == 0:
            src = tok.at[me]
            arr[tp, me] = tok[me]
        else:
            tok_copies[j - 1].wait_recv()
            src = arr.at[tp, s]
        c = remote(src, arr.at[tp, s], ty_send.at[j], ty_recv.at[j], me, tp_y)
        c.start()
        y_copies.append(c)
        c = remote(src, arr.at[tp, s], tc_send.at[0, j], tc_recv.at[0, j], me, tp_core)
        c.start()
        core_copies[0].append(c)

    def first_products(quarter):
        a = arr[quarter].reshape(total, width)
        deep = pl.ds(pl.multiple_of(quarter * width, width), width)
        return (
            jnp.dot(a, wg[deep, :], preferred_element_type=jnp.float32),
            jnp.dot(a, wu[deep, :], preferred_element_type=jnp.float32),
        )

    loads[0].wait()
    loads[1].wait()
    gate, up = first_products(tp)
    for c in core_copies[0]:
        c.wait_recv()
    more = first_products(tp_core)
    gate, up = gate + more[0], up + more[1]
    for j in range(n):
        s = source(j)
        y_copies[j].wait_recv()
        c = remote(
            arr.at[tp_y, s], arr.at[tp_y, s], tc_send.at[1, j], tc_recv.at[1, j], me, tp_core
        )
        c.start()
        core_copies[1].append(c)
    more = first_products(tp_y)
    gate, up = gate + more[0], up + more[1]
    for c in core_copies[1]:
        c.wait_recv()
    more = first_products(tp_both)
    gate, up = gate + more[0], up + more[1]
    sent += tok_copies + y_copies + core_copies[0] + core_copies[1]
    for j in range(1, n):
        s = source(j)
        unit_copies[0, j].wait_recv()
        c = remote(vbuf.at[side, s], vbuf.at[side, s], v_send.at[s], v_recv.at[s], pair, tp)
        c.start()
        v_copies.append(c)
    hidden = (jax.nn.silu(gate) * up).astype(jnp.bfloat16)

    loads[2].wait()
    order = (tp_both, tp_y, tp_core, tp)
    near_copies = []
    for i in range(4):
        cols = pl.ds(pl.multiple_of(order[i] * width, width), width)
        part[i] = (
            jnp.dot(hidden, wd[:, cols], preferred_element_type=jnp.float32)
            .astype(jnp.bfloat16)
            .reshape(n, slots, width)
        )
        if i % 2 == 0:
            h = i // 2
            c = remote(part.at[i], near.at[h], rc_send.at[h], rc_recv.at[h], me, tp_core)
            c.start()
            near_copies.append(c)
    near_copies[0].wait_recv()
    far_copies = []
    for j in range(n):
        d = peer(j)
        csum[d] = (part[1, d].astype(jnp.float32) + near[0, d].astype(jnp.float32)).astype(
            jnp.bfloat16
        )
        c = remote(csum.at[d], far.at[d], ry_send.at[j], ry_recv.at[j], me, tp_y)
        c.start()
        far_copies.append(c)
    sent += near_copies + far_copies
    near_copies[1].wait_recv()

    for j in range(1, n):
        unit_copies[1, j].wait_recv()
        unit_copies[2, j].wait_recv()
    for c in v_copies:
        c.wait_recv()
    sent += list(unit_copies.values()) + v_copies

    lam = lam_ref[head]
    keep = jnp.where(side == 0, 1.0, -lam)
    take = jnp.where(side == 0, -lam, 1.0)
    size = 2 * rows
    diag = (
        lax.broadcasted_iota(jnp.int32, (size, size), 1)
        <= lax.broadcasted_iota(jnp.int32, (size, size), 0)
    )
    back_copies = []

    def expert_back(j):
        d = peer(j)
        far_copies[j].wait_recv()
        val = (
            part[3, d].astype(jnp.float32)
            + near[1, d].astype(jnp.float32)
            + far[d].astype(jnp.float32)
        ).astype(jnp.bfloat16)
        if j == 0:
            ret[me] = val
        else:
            res[d] = val
            c = remote(res.at[d], ret.at[me], e_send.at[j], e_recv.at[j], d, tp)
            c.start()
            back_copies.append(c)

    swaps = []

    def finish(i):
        s = 2 * i + side
        swaps[i].wait_recv()
        mixed = keep * osend[s].astype(jnp.float32) + take * oret[i].astype(jnp.float32)
        scaled = mixed * lax.rsqrt(jnp.mean(mixed * mixed, axis=-1, keepdims=True) + head_eps)
        fin[i] = (scaled * gain_ref[...] * head_scale).astype(jnp.bfloat16)

        @pl.when(s != me)
        def _():
            remote(fin.at[i], att_in.at[head], f_send.at[i], f_recv.at[head], s, tp).start()

        @pl.when(s == me)
        def _():
            att_in[head] = fin[i]

    for i in range(n // 2):
        seen = (i + 1) * size
        q = qbuf[2 * i : 2 * i + 2].reshape(size, QKD)
        k = kbuf[0 : 2 * i + 2].reshape(seen, QKD)
        v = jnp.concatenate(
            [vbuf[half, 0 : 2 * i + 2].reshape(seen, VD // 2) for half in range(2)], axis=1
        )
        scores = lax.dot_general(
            q, k, (((1,), (1,)), ((), ())), preferred_element_type=jnp.float32
        ) * QKD ** (-0.5)
        last = jnp.where(diag, scores[:, i * size :], neg_big)
        scores = last if i == 0 else jnp.concatenate([scores[:, : i * size], last], axis=1)
        weights = jnp.exp(scores - jnp.max(scores, axis=-1, keepdims=True))
        bottom = jnp.sum(weights, axis=-1, keepdims=True)
        o = jnp.dot(weights.astype(jnp.bfloat16), v, preferred_element_type=jnp.float32) / bottom
        osend[2 * i : 2 * i + 2] = o.astype(jnp.bfloat16).reshape(2, rows, VD)
        c = remote(
            osend.at[2 * i + 1 - side], oret.at[i], o_send.at[i], o_recv.at[i], pair, tp
        )
        c.start()
        swaps.append(c)
        expert_back(2 * i)
        expert_back(2 * i + 1)
        if i > 0:
            finish(i - 1)
    finish(n // 2 - 1)
    sent += swaps + back_copies

    for h in range(heads):

        @pl.when(2 * h + side != me)
        def _(h=h):
            remote(
                fin.at[h], att_in.at[h], f_send.at[h], f_recv.at[h], 2 * h + side, tp
            ).wait()

        att_ref[:, h * VD : (h + 1) * VD] = att_in[h]

    for c in back_copies:
        c.wait_recv()
    first, second = upright(score_ref, 0), upright(score_ref, 1)
    top = jnp.maximum(first, second)
    raised = (jnp.exp(first - top), jnp.exp(second - top))
    returned = ret[...].reshape(total, width)
    combined = jnp.zeros(out_ref.shape, jnp.float32)
    for c in range(TOP):
        picked = jnp.dot(pick[c], returned, preferred_element_type=jnp.float32)
        combined = combined + raised[c] / (raised[0] + raised[1]) * picked
    out_ref[...] = combined.astype(jnp.bfloat16)
    for c in sent:
        c.wait_send()


def hand_over(att_ref, out_ref, att_to, out_to):
    att_to[...] = att_ref[...]
    out_to[...] = out_ref[...]


def local(
    queries,
    key_rows,
    values,
    lambdas,
    head_gain,
    tokens,
    moe_gain,
    routes,
    route_scores,
    w_gate,
    w_up,
    w_down,
):
    n = lax.axis_size("ep")
    heads = lambdas.shape[0]
    rows = queries.shape[0]
    rows_b, model = tokens.shape
    slots = 2 * TOP * rows_b // n
    width = model // 4
    ff = w_gate.shape[2]
    vmem = pl.BlockSpec(memory_space=pltpu.VMEM)
    hbm = pl.BlockSpec(memory_space=pl.ANY)
    smem = pl.BlockSpec(memory_space=pltpu.SMEM)
    bf16 = jnp.bfloat16
    dma = pltpu.SemaphoreType.DMA
    shapes = (
        jax.ShapeDtypeStruct(queries.shape, bf16),
        jax.ShapeDtypeStruct((rows_b, width), bf16),
    )
    held = pl.pallas_call(
        functools.partial(step_kernel, n, heads),
        out_shape=shapes,
        in_specs=[vmem, vmem, vmem, smem] + [vmem] * 5 + [hbm, hbm, hbm],
        out_specs=(vmem, vmem),
        scratch_shapes=[
            pltpu.VMEM((model, ff), bf16),
            pltpu.VMEM((model, ff), bf16),
            pltpu.VMEM((ff, model), bf16),
            pltpu.VMEM((n, rows, QKD), bf16),
            pltpu.VMEM((n, rows, QKD), bf16),
            pltpu.VMEM((2, n, rows, VD // 2), bf16),
            pltpu.VMEM((n, rows, VD), bf16),
            pltpu.VMEM((n // 2, rows, VD), bf16),
            pltpu.VMEM((n // 2, rows, VD), bf16),
            pltpu.VMEM((heads, rows, VD), bf16),
            pltpu.VMEM((TOP, rows_b, n * slots), bf16),
            pltpu.VMEM((n, slots, width), bf16),
            pltpu.VMEM((4, n, slots, width), bf16),
            pltpu.VMEM((4, n, slots, width), bf16),
            pltpu.VMEM((2, n, slots, width), bf16),
            pltpu.VMEM((n, slots, width), bf16),
            pltpu.VMEM((n, slots, width), bf16),
            pltpu.VMEM((n, slots, width), bf16),
            pltpu.VMEM((n, slots, width), bf16),
            dma((3,)),
            dma((n,)),
            dma((n,)),
            dma((n,)),
            dma((n,)),
            dma((2, n)),
            dma((2, n)),
            dma((3, n)),
            dma((3, n)),
            dma((n,)),
            dma((n,)),
            dma((n // 2,)),
            dma((n // 2,)),
            dma((n // 2,)),
            dma((n // 2,)),
            dma((2,)),
            dma((2,)),
            dma((n,)),
            dma((n,)),
            dma((n,)),
            dma((n,)),
        ],
        compiler_params=pltpu.CompilerParams(
            collective_id=0, has_side_effects=True, vmem_limit_bytes=56 * 1024 * 1024
        ),
    )(
        queries,
        key_rows,
        values,
        lambdas,
        head_gain[None, :],
        tokens,
        moe_gain[None, :],
        routes.T,
        route_scores.T,
        w_gate,
        w_up,
        w_down,
    )
    return tuple(
        pl.pallas_call(
            hand_over, out_shape=shapes, in_specs=[vmem, vmem], out_specs=(vmem, vmem)
        )(*held)
    )


def fits(mesh, head_count):
    n, parts = mesh.shape["ep"], mesh.shape["tp"]
    return parts == 4 and n % 2 == 0 and 2 * (head_count // parts) == n


def solution(mesh):
    def step(*args):
        body = local if fits(mesh, args[3].shape[0]) else local_general
        return sharded(mesh, body)(*args)

    return step


def sharded(mesh, body):
    return jax.shard_map(
        body,
        mesh=mesh,
        in_specs=(
            P("ep", "tp"),
            P("ep", "tp"),
            P("ep", "tp"),
            P("tp"),
            P(),
            P("ep", None),
            P(),
            P("ep", None),
            P("ep", None),
            P("ep", None, "tp"),
            P("ep", None, "tp"),
            P("ep", "tp", None),
        ),
        out_specs=(P("ep", "tp"), P("ep", "tp")),
        check_vma=False,
    )
```

profile of v0, /device:TPU:25, one launch (start us, length us, event | category | flops | bytes accessed | tf_op | source)
XLA Modules:
  0.0 63.5 jit_solution(9924183119953096533)
XLA Ops:
  0.6 61.1 %shard_map.131 = (bf16[128,1024]{1,0:T(8,128)(2,1)}, bf16[64,1024]{1,0:T(8,128)(2,1)}) custom-call(bf16[128,1024]{1,0:T(8,128)(2,1)} %q_ref.1, bf16[128,1024]{1,0:T(8,128)(2,1)} %k_ref.1, bf16[128,1024]{1,0:T(8,128)(2,1)} %v_ref.1, f32[4]{0:T(128)} %lam_ref.1, f32[1,256]{1,0:T(1,128)} %bitcast.5, bf16[64,4096]{1,0:T(8,128)(2,1)} %tokens_ref.1, ...), custom_call_target="tpu_custom_call" | custom-call | tf_op jit(solution)/shard_map/pallas_call | solution.py:548
  61.8 1.7 %shard_map.132 = (bf16[128,1024]{1,0:T(8,128)(2,1)}, bf16[64,1024]{1,0:T(8,128)(2,1)}) custom-call(bf16[128,1024]{1,0:T(8,128)(2,1)} %get-tuple-element.4.att_ref, bf16[64,1024]{1,0:T(8,128)(2,1)} %get-tuple-element.5.out_ref), custom_call_target="tpu_custom_call" | custom-call | tf_op jit(solution)/shard_map/pallas_call | solution.py:613
where the time goes:
time: 63.7 us; the launch traced here: 63.5 us
  Pallas kernels  62.9 us (99%)
  between operations  0.64 us (1%)
    pallas_call x1, Pallas kernels, local(): pl.pallas_call(functools.partial(step_kernel, n, heads), out_shape=shapes...  61.1 us
    pallas_call x1, Pallas kernels, local(): pl.pallas_call(hand_over, out_shape=shapes, in_specs=[vmem, vmem], out_sp...  1.74 us

commit v1 on v0

v1 whole, which is shorter than its diff:
```python
import functools

import jax
import jax.numpy as jnp
from jax import lax
from jax.experimental import pallas as pl
from jax.experimental.pallas import tpu as pltpu
from jax.sharding import PartitionSpec as P

QKD = 128
VD = 256
TOP = 2


neg_big = -1e30
head_eps = 1e-05
moe_eps = 1e-06
head_scale = 0.8


def slot_table(routes, experts, capacity):
    flat_routes = routes.reshape(-1)
    onehot = (flat_routes[:, None] == jnp.arange(experts, dtype=jnp.int32)[None, :]).astype(
        jnp.int32
    )
    before = jnp.cumsum(onehot, axis=0) - onehot
    position = jnp.sum(before * onehot, axis=1)
    return (flat_routes * capacity + position).reshape(routes.shape)


def fold_block(state, query_group, query_pos, key_heads, value_heads, key_pos):
    maxima, denominators, accumulated = state
    scores = jnp.einsum(
        "qhmd,khmd->hmqk", query_group, key_heads, preferred_element_type=jnp.float32
    ) * QKD ** (-0.5)
    visible = key_pos[None, :] <= query_pos[:, None]
    scores = jnp.where(visible, scores, neg_big)
    new_max = jnp.maximum(maxima, jnp.max(scores, axis=-1))
    weights = jnp.where(visible, jnp.exp(scores - new_max[..., None]), 0.0)
    accumulated = jnp.einsum(
        "hmqk,khd->hmqd", weights, value_heads, precision=lax.Precision.HIGHEST
    )
    denominators = jnp.sum(weights, axis=-1)
    return (new_max, denominators, accumulated)


def local_general(
    queries,
    key_rows,
    values,
    lambdas,
    head_gain,
    tokens,
    moe_gain,
    routes,
    route_scores,
    w_gate,
    w_up,
    w_down,
):
    rows_a = queries.shape[0]
    half_rows = rows_a // 2
    head_local = lambdas.shape[0]
    ep_count = lax.axis_size("ep")
    ep_index = lax.axis_index("ep")
    early_queries = queries[:half_rows]
    later_queries = queries[half_rows:]
    early_pos = ep_index * rows_a + jnp.arange(half_rows, dtype=jnp.int32)
    later_pos = ep_index * rows_a + half_rows + jnp.arange(half_rows, dtype=jnp.int32)
    query_groups = (
        early_queries.reshape(half_rows, head_local, 2, QKD),
        later_queries.reshape(half_rows, head_local, 2, QKD),
    )
    position_groups = (early_pos, later_pos)
    start_state = (
        jnp.full((head_local, 2, half_rows), neg_big, jnp.float32),
        jnp.zeros((head_local, 2, half_rows), jnp.float32),
        jnp.zeros((head_local, 2, half_rows, VD), jnp.float32),
    )
    totals = (start_state, start_state)
    row_start = jnp.int32(0)
    key_block = lax.all_gather(key_rows, "ep", axis=0, tiled=True)
    value_block = lax.all_gather(values, "ep", axis=0, tiled=True)
    key_count = key_block.shape[0]
    key_heads = key_block.reshape(key_count, head_local, 2, QKD)
    value_heads = value_block.reshape(key_count, head_local, VD).astype(jnp.float32)
    key_pos = jnp.arange(key_count, dtype=jnp.int32)
    updated = []
    for attend_group_index in range(2):
        state = totals[attend_group_index]
        query_group = query_groups[attend_group_index]
        query_pos = position_groups[attend_group_index]
        state = lax.cond(
            row_start <= query_pos[-1],
            lambda held: fold_block(held, query_group, query_pos, key_heads, value_heads, key_pos),
            lambda held: held,
            state,
        )
        updated.append(state)
    folded = (updated[0], updated[1])
    attended_groups = []
    for group_index in range(2):
        maxima, denominators, accumulated = folded[group_index]
        mixed_out = (
            accumulated[:, 0] / denominators[:, 0, :, None]
            - lambdas[:, None, None] * accumulated[:, 1] / denominators[:, 1, :, None]
        )
        scaled = mixed_out * lax.rsqrt(
            jnp.mean(mixed_out * mixed_out, axis=-1, keepdims=True) + head_eps
        )
        scaled = scaled * head_gain * head_scale
        attended_groups.append(
            scaled.transpose(1, 0, 2).reshape(half_rows, head_local * VD).astype(jnp.bfloat16)
        )
    later_out = attended_groups[1]
    attended = jnp.concatenate([attended_groups[0], later_out], axis=0)
    rows_b = tokens.shape[0]
    capacity = 2 * TOP * rows_b // ep_count
    token_f32 = tokens.astype(jnp.float32)
    normed = (
        token_f32
        * lax.rsqrt(jnp.mean(token_f32 * token_f32, axis=-1, keepdims=True) + moe_eps)
        * moe_gain
    ).astype(jnp.bfloat16)
    gate_weights = jax.nn.softmax(route_scores, axis=-1)
    slot_of = slot_table(routes, ep_count, capacity)
    row_ids = jnp.broadcast_to(jnp.arange(rows_b, dtype=jnp.int32)[:, None], slot_of.shape)
    row_of_slot = (
        jnp.zeros((ep_count * capacity,), jnp.int32)
        .at[slot_of.reshape(-1)]
        .set(row_ids.reshape(-1))
    )
    gate_local = w_gate[0]
    up_local = w_up[0]
    down_local = w_down[0]
    outgoing = normed[row_of_slot]
    arrived = lax.all_to_all(outgoing, "ep", split_axis=0, concat_axis=0, tiled=True)
    gate_act = jnp.dot(arrived, gate_local, preferred_element_type=jnp.float32)
    up_act = jnp.dot(arrived, up_local, preferred_element_type=jnp.float32)
    hidden = (jax.nn.silu(gate_act) * up_act).astype(jnp.bfloat16)
    summed = lax.psum_scatter(
        lax.dot_general(
            down_local, hidden, (((0,), (1,)), ((), ())), preferred_element_type=jnp.float32
        ).astype(jnp.bfloat16),
        "tp",
        scatter_dimension=0,
        tiled=True,
    )
    returned = lax.all_to_all(summed, "ep", split_axis=1, concat_axis=1, tiled=True)
    slot_ids = jnp.arange(ep_count * capacity, dtype=jnp.int32)
    combined = jnp.zeros((rows_b, returned.shape[0]), jnp.float32)
    for choice_index in range(TOP):
        picker = (slot_of[:, choice_index, None] == slot_ids[None, :]).astype(jnp.bfloat16)
        picked = lax.dot_general(
            picker, returned, (((1,), (1,)), ((), ())), preferred_element_type=jnp.float32
        )
        combined = combined + gate_weights[:, choice_index, None] * picked
    expert_out = combined.astype(jnp.bfloat16)
    return (attended, expert_out)


MESH = pl.DeviceIdType.MESH


def step_kernel(
    n,
    heads,
    q_in,
    k_in,
    v_in,
    lam_ref,
    gain_ref,
    tokens_in,
    moe_gain_ref,
    routes_ref,
    score_ref,
    wg_ref,
    wu_ref,
    wd_ref,
    att_ref,
    out_ref,
    wg,
    wu,
    wd,
    qb,
    kb,
    vb,
    qm,
    pr,
    stat_out,
    stat_in,
    osend,
    oret,
    fin,
    att_in,
    routes_m,
    score_m,
    dense,
    dense_m,
    pick,
    tok,
    arr,
    part,
    near,
    csum,
    far,
    res,
    ret,
    back,
    back_m,
    q_ref,
    k_ref,
    v_ref,
    tokens_ref,
    w_sem,
    m_send,
    m_recv,
    tok_send,
    tok_recv,
    ty_send,
    ty_recv,
    tc_send,
    tc_recv,
    a_send,
    a_recv,
    qm_send,
    qm_recv,
    x_send,
    x_recv,
    f_send,
    f_recv,
    rc_send,
    rc_recv,
    ry_send,
    ry_recv,
    e_send,
    e_recv,
):
    me = lax.axis_index("ep")
    tp = lax.axis_index("tp")
    y = tp // 2
    core = tp % 2
    tp_core = y * 2 + 1 - core
    tp_y = (1 - y) * 2 + core
    tp_both = (1 - y) * 2 + 1 - core
    g = n // 2
    half = me // g
    w = me % g
    base = half * g
    mirror = (1 - half) * g + w
    rows = q_ref.shape[0]
    rows_b = tokens_ref.shape[0]
    slots, width = tok.shape[2:]
    total = g * slots

    def ahead(j):
        return lax.rem(w + j, g)

    def behind(j):
        return lax.rem(w + g - j, g)

    def remote(src, dst, send, recv, ep, tpi):
        return pltpu.make_async_remote_copy(
            src_ref=src,
            dst_ref=dst,
            send_sem=send,
            recv_sem=recv,
            device_id=(ep, tpi),
            device_id_type=MESH,
        )

    barrier = pltpu.get_barrier_semaphore()
    for j in range(1, g):
        pl.semaphore_signal(barrier, inc=1, device_id=(base + ahead(j), tp), device_id_type=MESH)
    pl.semaphore_signal(barrier, inc=1, device_id=(mirror, tp), device_id_type=MESH)
    pl.semaphore_signal(barrier, inc=1, device_id=(me, tp_core), device_id_type=MESH)
    pl.semaphore_signal(barrier, inc=1, device_id=(me, tp_y), device_id_type=MESH)
    staged = [
        pltpu.make_async_copy(src, dst, w_sem.at[3 + i])
        for i, (src, dst) in enumerate(
            ((tokens_in, tokens_ref), (q_in, q_ref), (k_in, k_ref), (v_in, v_ref))
        )
    ]
    for c in staged:
        c.start()
    loads = [
        pltpu.make_async_copy(wg_ref.at[0], wg, w_sem.at[0]),
        pltpu.make_async_copy(wu_ref.at[0], wu, w_sem.at[1]),
        pltpu.make_async_copy(wd_ref.at[0], wd, w_sem.at[2]),
    ]
    for load in loads:
        load.start()

    features = pl.ds(pl.multiple_of(tp * width, width), width)
    staged[0].wait()
    token_f32 = tokens_ref[...].astype(jnp.float32)
    inverse = lax.rsqrt(jnp.mean(token_f32 * token_f32, axis=-1, keepdims=True) + moe_eps)
    dense[...] = (
        tokens_ref[:, features].astype(jnp.float32) * inverse * moe_gain_ref[:, features]
    ).astype(jnp.bfloat16)
    lane = lax.broadcasted_iota(jnp.int32, (rows_b, 128), 1)
    square = (rows_b, rows_b)
    row_at = lax.broadcasted_iota(jnp.int32, square, 0)
    column_at = lax.broadcasted_iota(jnp.int32, square, 1)
    below = jnp.where(column_at < row_at, 1.0, 0.0).astype(jnp.bfloat16)
    slot_ids = lax.broadcasted_iota(jnp.int32, (rows_b, total), 1).astype(jnp.float32)

    def upright(ref, c):
        line = jnp.broadcast_to(ref[c : c + 1, :], square)
        return jnp.sum(
            jnp.where(row_at == column_at, line, jnp.zeros_like(line)), axis=1, keepdims=True
        )

    def choose(group, ref, source):
        named_by = [upright(ref, c) for c in range(TOP)]
        named = [named_by[c] == lane for c in range(TOP)]
        either = jnp.where(named[0] | named[1], 1.0, 0.0).astype(jnp.bfloat16)
        before = jnp.dot(below, either, preferred_element_type=jnp.float32)
        chosen = jnp.zeros((rows_b, total), jnp.float32)
        for c in range(TOP):
            position = jnp.sum(jnp.where(named[c], before, 0.0), axis=1, keepdims=True)
            slot = (named_by[c] - base).astype(jnp.float32) * slots + position
            hit = jnp.where(slot == slot_ids, 1.0, 0.0)
            pick[group, c] = hit.astype(jnp.bfloat16)
            chosen = chosen + hit
        tok[group] = (
            jnp.dot(
                chosen.T.astype(jnp.bfloat16), source[...], preferred_element_type=jnp.float32
            )
            .astype(jnp.bfloat16)
            .reshape(g, slots, width)
        )

    choose(0, routes_ref, dense)
    pl.semaphore_wait(barrier, g + 2)

    for c in staged[1:]:
        c.wait()
    sent = []
    mirrored = [
        remote(routes_ref, routes_m, m_send.at[0], m_recv.at[0], mirror, tp),
        remote(score_ref, score_m, m_send.at[1], m_recv.at[1], mirror, tp),
        remote(dense, dense_m, m_send.at[2], m_recv.at[2], mirror, tp),
    ]
    for c in mirrored:
        c.start()
    sent += mirrored
    tok_copies = {}

    def scatter(group):
        for j in range(1, g):
            d = ahead(j)
            c = remote(
                tok.at[group, d],
                arr.at[tp, group, w],
                tok_send.at[group, j],
                tok_recv.at[group, j],
                base + d,
                tp,
            )
            c.start()
            tok_copies[group, j] = c

    unit_copies = {}

    def share(which, src, dst):
        for j in range(1, g):
            d = ahead(j)
            cols = pl.ds(pl.multiple_of(d * VD, VD), VD)
            c = remote(
                src.at[:, cols],
                dst.at[w],
                a_send.at[which, j],
                a_recv.at[which, j],
                base + d,
                tp,
            )
            c.start()
            unit_copies[which, j] = c

    y_copies, core_copies, more_copies = {}, {}, {}

    def hand(group, j):
        s = behind(j)
        if j == 0:
            src = tok.at[group, w]
            arr[tp, group, w] = tok[group, w]
        else:
            tok_copies[group, j].wait_recv()
            src = arr.at[tp, group, s]
        c = remote(
            src, arr.at[tp, group, s], ty_send.at[group, j], ty_recv.at[group, j], me, tp_y
        )
        c.start()
        y_copies[group, j] = c
        c = remote(
            src,
            arr.at[tp, group, s],
            tc_send.at[0, group, j],
            tc_recv.at[0, group, j],
            me,
            tp_core,
        )
        c.start()
        core_copies[group, j] = c

    scatter(0)
    share(1, q_ref, qb)
    hand(0, 0)
    own = pl.ds(pl.multiple_of(w * VD, VD), VD)
    kb[w] = k_ref[:, own]
    qb[w] = q_ref[:, own]
    vb[w] = v_ref[:, own]
    for j in range(1, g):
        hand(0, j)
    for c in mirrored:
        c.wait_recv()
    choose(1, routes_m, dense_m)
    scatter(1)
    hand(1, 0)
    def q_on(s):
        return remote(qb.at[s], qm.at[s], qm_send.at[s], qm_recv.at[s], mirror, tp)

    @pl.when(half == 1)
    def _():
        for j in range(1, g):
            unit_copies[1, j].wait_recv()
        for s in range(g):
            q_on(s).start()

    share(0, k_ref, kb)
    share(2, v_ref, vb)

    def first_products(group, quarter):
        a = arr[quarter, group].reshape(total, width)
        deep = pl.ds(pl.multiple_of(quarter * width, width), width)
        return (
            jnp.dot(a, wg[deep, :], preferred_element_type=jnp.float32),
            jnp.dot(a, wu[deep, :], preferred_element_type=jnp.float32),
        )

    def near_half(group):
        one = first_products(group, tp)
        for j in range(g):
            core_copies[group, j].wait_recv()
        two = first_products(group, tp_core)
        return one[0] + two[0], one[1] + two[1]

    order = (tp_both, tp_y, tp_core, tp)
    near_copies, far_copies = {}, {}

    def far_half(group, gate, up):
        for j in range(g):
            s = behind(j)
            y_copies[group, j].wait_recv()
            c = remote(
                arr.at[tp_y, group, s],
                arr.at[tp_y, group, s],
                tc_send.at[1, group, j],
                tc_recv.at[1, group, j],
                me,
                tp_core,
            )
            c.start()
            more_copies[group, j] = c
        more = first_products(group, tp_y)
        gate, up = gate + more[0], up + more[1]
        for j in range(g):
            more_copies[group, j].wait_recv()
        more = first_products(group, tp_both)
        gate, up = gate + more[0], up + more[1]
        return (jax.nn.silu(gate) * up).astype(jnp.bfloat16)

    def second_products(group, hidden):
        for i in range(4):
            cols = pl.ds(pl.multiple_of(order[i] * width, width), width)
            part[group, i] = (
                jnp.dot(hidden, wd[:, cols], preferred_element_type=jnp.float32)
                .astype(jnp.bfloat16)
                .reshape(g, slots, width)
            )
            if i % 2 == 0:
                h = i // 2
                c = remote(
                    part.at[group, i],
                    near.at[group, h],
                    rc_send.at[group, h],
                    rc_recv.at[group, h],
                    me,
                    tp_core,
                )
                c.start()
                near_copies[group, h] = c
        near_copies[group, 0].wait_recv()
        for j in range(g):
            d = ahead(j)
            csum[group, d] = (
                part[group, 1, d].astype(jnp.float32) + near[group, 0, d].astype(jnp.float32)
            ).astype(jnp.bfloat16)
            c = remote(
                csum.at[group, d],
                far.at[group, d],
                ry_send.at[group, j],
                ry_recv.at[group, j],
                me,
                tp_y,
            )
            c.start()
            far_copies[group, j] = c

    back_copies = {}

    def expert_back(group):
        near_copies[group, 1].wait_recv()
        for j in range(g):
            d = ahead(j)
            far_copies[group, j].wait_recv()
            val = (
                part[group, 3, d].astype(jnp.float32)
                + near[group, 1, d].astype(jnp.float32)
                + far[group, d].astype(jnp.float32)
            ).astype(jnp.bfloat16)
            if j == 0:
                ret[group, w] = val
            else:
                res[group, d] = val
                c = remote(
                    res.at[group, d],
                    ret.at[group, w],
                    e_send.at[group, j],
                    e_recv.at[group, j],
                    base + d,
                    tp,
                )
                c.start()
                back_copies[group, j] = c

    def combine(group, ref):
        for j in range(1, g):
            back_copies[group, j].wait_recv()
        first, second = upright(ref, 0), upright(ref, 1)
        top = jnp.maximum(first, second)
        raised = (jnp.exp(first - top), jnp.exp(second - top))
        returned = ret[group].reshape(total, width)
        combined = jnp.zeros(out_ref.shape, jnp.float32)
        for c in range(TOP):
            picked = jnp.dot(pick[group, c], returned, preferred_element_type=jnp.float32)
            combined = combined + raised[c] / (raised[0] + raised[1]) * picked
        return combined

    loads[0].wait()
    loads[1].wait()
    gate, up = near_half(0)
    hidden = far_half(0, gate, up)
    for j in range(1, g):
        hand(1, j)
    loads[2].wait()
    second_products(0, hidden)
    lam = lam_ref[w]
    size = 2 * rows
    blocks = g // 2
    reach = g * rows
    diag = (
        lax.broadcasted_iota(jnp.int32, (size, size), 1)
        <= lax.broadcasted_iota(jnp.int32, (size, size), 0)
    )
    stat_lane = lax.broadcasted_iota(jnp.int32, (size, 128), 1)

    def weigh(q, seen, masked):
        found = []
        for m in range(2):
            cols = slice(m * QKD, (m + 1) * QKD)
            k = kb[0 : seen // rows].reshape(seen, 2 * QKD)[:, cols]
            scores = lax.dot_general(
                q[:, cols], k, (((1,), (1,)), ((), ())), preferred_element_type=jnp.float32
            ) * QKD ** (-0.5)
            if masked:
                last = jnp.where(diag, scores[:, seen - size :], neg_big)
                scores = (
                    last
                    if seen == size
                    else jnp.concatenate([scores[:, : seen - size], last], axis=1)
                )
            top = jnp.max(scores, axis=-1, keepdims=True)
            weights = jnp.exp(scores - top)
            found.append((weights, top, jnp.sum(weights, axis=-1, keepdims=True)))
        return found

    def blend(first, second, one, two, seen):
        v = vb[0 : seen // rows].reshape(seen, VD)
        mixed = (first * one - second * two).astype(jnp.bfloat16)
        return jnp.dot(mixed, v, preferred_element_type=jnp.float32)

    def keep(i, seen, found):
        (one, top_one, sum_one), (two, top_two, sum_two) = found
        line = pl.ds(i * size, size)
        pr[0, line, 0:seen] = one
        pr[1, line, 0:seen] = two
        packed = jnp.where(
            stat_lane == 0,
            top_one,
            jnp.where(stat_lane == 1, sum_one, jnp.where(stat_lane == 2, top_two, sum_two)),
        )
        stat_out[:, line] = packed.T[0:8]

    def stats_on():
        return remote(stat_out, stat_in, x_send.at[0], x_recv.at[0], mirror, tp)

    def o_on(i):
        line = pl.ds(i * size, size)
        return remote(
            osend.at[line], oret.at[line], x_send.at[1 + i], x_recv.at[1 + i], mirror, tp
        )

    def merged():
        mine, other = stat_out[...], stat_in[...]
        scale = []
        for m in range(2):
            top, bottom = mine[2 * m : 2 * m + 1], mine[2 * m + 1 : 2 * m + 2]
            top_o, bottom_o = other[2 * m : 2 * m + 1], other[2 * m + 1 : 2 * m + 2]
            high = jnp.maximum(top, top_o)
            part_mine = jnp.exp(top - high)
            scale.append(part_mine / (bottom * part_mine + bottom_o * jnp.exp(top_o - high)))
        at = lax.broadcasted_iota(jnp.int32, (128, reach), 0)
        both = jnp.where(at == 0, scale[0], jnp.where(at == 1, scale[1] * lam, 0.0))
        return both.T

    def f_on(d):
        return remote(fin.at[d], att_in.at[w], f_send.at[d], f_recv.at[w], base + d, tp)

    def finish(i, mixed):
        scaled = mixed * lax.rsqrt(jnp.mean(mixed * mixed, axis=-1, keepdims=True) + head_eps)
        scaled = (scaled * gain_ref[...] * head_scale).astype(jnp.bfloat16)
        fin[2 * i : 2 * i + 2] = scaled.reshape(2, rows, VD)
        for d in (2 * i, 2 * i + 1):

            @pl.when(d != w)
            def _(d=d):
                f_on(d).start()

            @pl.when(d == w)
            def _(d=d):
                att_in[w] = fin[d]

    gate, up = near_half(1)
    hidden = far_half(1, gate, up)
    second_products(1, hidden)

    for j in range(1, g):
        unit_copies[0, j].wait_recv()

    @pl.when(half == 1)
    def _():
        for i in range(blocks):
            q = qb[2 * i : 2 * i + 2].reshape(size, 2 * QKD)
            seen = (i + 1) * size
            keep(i, seen, weigh(q, seen, True))
        stats_on().start()

    @pl.when(half == 0)
    def _():
        for s in range(g):
            q_on(s).wait_recv()
        for i in range(blocks):
            q = qm[2 * i : 2 * i + 2].reshape(size, 2 * QKD)
            keep(i, reach, weigh(q, reach, False))
        stats_on().start()

    for j in range(1, g):
        unit_copies[2, j].wait_recv()
    stats_on().wait_recv()
    scales = merged()

    @pl.when(half == 0)
    def _():
        for i in range(blocks):
            line = pl.ds(i * size, size)
            part_scale = scales[i * size : (i + 1) * size]
            osend[line] = blend(
                pr[0, line], pr[1, line], part_scale[:, 0:1], part_scale[:, 1:2], reach
            ).astype(jnp.bfloat16)
            o_on(i).start()

    expert_back(0)

    @pl.when(half == 0)
    def _():
        for j in range(1, g):
            unit_copies[1, j].wait_recv()
        for i in range(blocks):
            q = qb[2 * i : 2 * i + 2].reshape(size, 2 * QKD)
            seen = (i + 1) * size
            one, two = weigh(q, seen, True)
            finish(i, blend(one[0], two[0], 1.0 / one[2], lam / two[2], seen))

    expert_back(1)
    back[...] = combine(1, score_m).astype(jnp.bfloat16)
    last = remote(back, back_m, m_send.at[3], m_recv.at[3], mirror, tp)
    last.start()
    sent.append(last)

    @pl.when(half == 1)
    def _():
        for i in range(blocks):
            line = pl.ds(i * size, size)
            seen = (i + 1) * size
            part_scale = scales[i * size : (i + 1) * size]
            mixed = blend(
                pr[0, line, 0:seen],
                pr[1, line, 0:seen],
                part_scale[:, 0:1],
                part_scale[:, 1:2],
                seen,
            )
            o_on(i).wait_recv()
            finish(i, mixed + oret[line].astype(jnp.float32))

    combined = combine(0, score_ref)

    for h in range(heads):

        @pl.when(h != w)
        def _(h=h):
            remote(fin.at[h], att_in.at[h], f_send.at[h], f_recv.at[h], base + h, tp).wait()

        att_ref[:, h * VD : (h + 1) * VD] = att_in[h]

    last.wait_recv()
    out_ref[...] = (combined + back_m[...].astype(jnp.float32)).astype(jnp.bfloat16)

    @pl.when(half == 1)
    def _():
        for s in range(g):
            q_on(s).wait_send()

    @pl.when(half == 0)
    def _():
        for i in range(blocks):
            o_on(i).wait_send()

    stats_on().wait_send()
    for group in (
        tok_copies,
        unit_copies,
        y_copies,
        core_copies,
        more_copies,
        near_copies,
        far_copies,
        back_copies,
    ):
        sent += list(group.values())
    for c in sent:
        c.wait_send()


def local(
    queries,
    key_rows,
    values,
    lambdas,
    head_gain,
    tokens,
    moe_gain,
    routes,
    route_scores,
    w_gate,
    w_up,
    w_down,
):
    n = lax.axis_size("ep")
    heads = lambdas.shape[0]
    rows = queries.shape[0]
    rows_b, model = tokens.shape
    slots = 2 * TOP * rows_b // n
    width = model // 4
    ff = w_gate.shape[2]
    vmem = pl.BlockSpec(memory_space=pltpu.VMEM)
    hbm = pl.BlockSpec(memory_space=pl.ANY)
    smem = pl.BlockSpec(memory_space=pltpu.SMEM)
    bf16, f32 = jnp.bfloat16, jnp.float32
    g = n // 2
    dma = pltpu.SemaphoreType.DMA
    shapes = (
        jax.ShapeDtypeStruct(queries.shape, bf16),
        jax.ShapeDtypeStruct((rows_b, width), bf16),
    )
    inside = (pltpu.VMEM(queries.shape, bf16), pltpu.VMEM((rows_b, width), bf16))
    held = pl.pallas_call(
        functools.partial(step_kernel, n, heads),
        out_shape=inside,
        in_specs=[hbm, hbm, hbm, smem, vmem, hbm] + [vmem] * 3 + [hbm, hbm, hbm],
        out_specs=(vmem, vmem),
        scratch_shapes=[
            pltpu.VMEM((model, ff), bf16),
            pltpu.VMEM((model, ff), bf16),
            pltpu.VMEM((ff, model), bf16),
            pltpu.VMEM((g, rows, VD), bf16),
            pltpu.VMEM((g, rows, VD), bf16),
            pltpu.VMEM((g, rows, VD), bf16),
            pltpu.VMEM((g, rows, VD), bf16),
            pltpu.VMEM((2, g * rows, g * rows), f32),
            pltpu.VMEM((8, g * rows), f32),
            pltpu.VMEM((8, g * rows), f32),
            pltpu.VMEM((g * rows, VD), bf16),
            pltpu.VMEM((g * rows, VD), bf16),
            pltpu.VMEM((g, rows, VD), bf16),
            pltpu.VMEM((heads, rows, VD), bf16),
            pltpu.VMEM((TOP, rows_b), jnp.int32),
            pltpu.VMEM((TOP, rows_b), f32),
            pltpu.VMEM((rows_b, width), bf16),
            pltpu.VMEM((rows_b, width), bf16),
            pltpu.VMEM((2, TOP, rows_b, g * slots), bf16),
            pltpu.VMEM((2, g, slots, width), bf16),
            pltpu.VMEM((4, 2, g, slots, width), bf16),
            pltpu.VMEM((2, 4, g, slots, width), bf16),
            pltpu.VMEM((2, 2, g, slots, width), bf16),
            pltpu.VMEM((2, g, slots, width), bf16),
            pltpu.VMEM((2, g, slots, width), bf16),
            pltpu.VMEM((2, g, slots, width), bf16),
            pltpu.VMEM((2, g, slots, width), bf16),
            pltpu.VMEM((rows_b, width), bf16),
            pltpu.VMEM((rows_b, width), bf16),
            pltpu.VMEM(queries.shape, bf16),
            pltpu.VMEM(queries.shape, bf16),
            pltpu.VMEM(queries.shape, bf16),
            pltpu.VMEM(tokens.shape, bf16),
            dma((7,)),
            dma((4,)),
            dma((4,)),
            dma((2, g)),
            dma((2, g)),
            dma((2, g)),
            dma((2, g)),
            dma((2, 2, g)),
            dma((2, 2, g)),
            dma((3, g)),
            dma((3, g)),
            dma((g,)),
            dma((g,)),
            dma((1 + g // 2,)),
            dma((1 + g // 2,)),
            dma((g,)),
            dma((g,)),
            dma((2, 2)),
            dma((2, 2)),
            dma((2, g)),
            dma((2, g)),
            dma((2, g)),
            dma((2, g)),
        ],
        compiler_params=pltpu.CompilerParams(
            collective_id=0, has_side_effects=True, vmem_limit_bytes=56 * 1024 * 1024
        ),
    )(
        queries,
        key_rows,
        values,
        lambdas,
        head_gain[None, :],
        tokens,
        moe_gain[None, :],
        routes.T,
        route_scores.T,
        w_gate,
        w_up,
        w_down,
    )
    return tuple(held)


def fits(mesh, head_count):
    n, parts = mesh.shape["ep"], mesh.shape["tp"]
    return parts == 4 and n % 2 == 0 and 2 * (head_count // parts) == n


def solution(mesh):
    def step(*args):
        body = local if fits(mesh, args[3].shape[0]) else local_general
        return sharded(mesh, body)(*args)

    return step


def sharded(mesh, body):
    return jax.shard_map(
        body,
        mesh=mesh,
        in_specs=(
            P("ep", "tp"),
            P("ep", "tp"),
            P("ep", "tp"),
            P("tp"),
            P(),
            P("ep", None),
            P(),
            P("ep", None),
            P("ep", None),
            P("ep", None, "tp"),
            P("ep", None, "tp"),
            P("ep", "tp", None),
        ),
        out_specs=(P("ep", "tp"), P("ep", "tp")),
        check_vma=False,
    )
```

time: 63.7 us -> 55.8 us (0.88)
  the two profiles are of different devices: /device:TPU:25 before, /device:TPU:26 now
where the time goes in v1:
time: 55.8 us; the launch traced here: 55.6 us
  Pallas kernels  53.6 us (96%)
  local copies, waits for them, and re-layouts  1.36 us (2%)
  between operations  0.64 us (1%)
    pallas_call x1, Pallas kernels, local(): pl.pallas_call(functools.partial(step_kernel, n, heads), out_shape=inside...  53.6 us
    unnamed x2, local copies, waits for them, and re-layouts  1.36 us

profile of v1, /device:TPU:26, one launch (start us, length us, event | category | flops | bytes accessed | tf_op | source)
XLA Modules:
  0.0 55.6 jit_solution(9240190253281938439)
XLA Ops:
  0.6 53.6 %shard_map.131 = (bf16[128,1024]{1,0:T(8,128)(2,1)S(1)}, bf16[64,1024]{1,0:T(8,128)(2,1)S(1)}) custom-call(bf16[128,1024]{1,0:T(8,128)(2,1)} %q_in.1, bf16[128,1024]{1,0:T(8,128)(2,1)} %k_in.1, bf16[128,1024]{1,0:T(8,128)(2,1)} %v_in.1, f32[4]{0:T(128)} %lam_ref.1, f32[1,256]{1,0:T(1,128)} %bitcast.5, bf16[64,4096]{1,0:T(8,128)(2,1)} %tokens_in.1, ...), custom_call_target="tpu_custom_call" | custom-call | tf_op jit(solution)/shard_map/pallas_call | solution.py:789
  54.2 0.7 %copy.16 = bf16[128,1024]{1,0:T(8,128)(2,1)} copy(bf16[128,1024]{1,0:T(8,128)(2,1)S(1)} %get-tuple-element.2) | data formatting | bytes 524288
  54.9 0.7 %copy.17 = bf16[64,1024]{1,0:T(8,128)(2,1)} copy(bf16[64,1024]{1,0:T(8,128)(2,1)S(1)} %get-tuple-element.3) | data formatting | bytes 262144

commit v2 on v1

--- a/solution.py
+++ b/solution.py
@@ -168,12 +168,12 @@
     q_in,
     k_in,
     v_in,
-    lam_ref,
-    gain_ref,
+    lam_in,
+    gain_in,
     tokens_in,
-    moe_gain_ref,
-    routes_ref,
-    score_ref,
+    moe_gain_in,
+    routes_in,
+    score_in,
     wg_ref,
     wu_ref,
     wd_ref,
@@ -182,15 +182,16 @@
     wg,
     wu,
     wd,
-    qb,
-    kb,
-    vb,
+    qx,
+    kk,
+    vv,
     qm,
     pr,
     stat_out,
     stat_in,
     osend,
     oret,
+    olate,
     fin,
     att_in,
     routes_m,
@@ -212,6 +213,11 @@
     k_ref,
     v_ref,
     tokens_ref,
+    lam_ref,
+    gain_ref,
+    moe_gain_ref,
+    routes_ref,
+    score_ref,
     w_sem,
     m_send,
     m_recv,
@@ -223,10 +229,14 @@
     tc_recv,
     a_send,
     a_recv,
+    kv_send,
+    kv_recv,
     qm_send,
     qm_recv,
-    x_send,
-    x_recv,
+    st_send,
+    st_recv,
+    o_send,
+    o_recv,
     f_send,
     f_recv,
     rc_send,
@@ -248,16 +258,17 @@
     w = me % g
     base = half * g
     mirror = (1 - half) * g + w
+    level = me // 2
+    x = me % 2
+    high = level % 2
+    beside = level * 2 + 1 - x
     rows = q_ref.shape[0]
     rows_b = tokens_ref.shape[0]
     slots, width = tok.shape[2:]
     total = g * slots
 
     def ahead(j):
-        return lax.rem(w + j, g)
-
-    def behind(j):
-        return lax.rem(w + g - j, g)
+        return (w, lax.rem(w + g // 2, g), g - 1 - w, w + 1 - 2 * x)[j]
 
     def remote(src, dst, send, recv, ep, tpi):
         return pltpu.make_async_remote_copy(
@@ -273,12 +284,35 @@
     for j in range(1, g):
         pl.semaphore_signal(barrier, inc=1, device_id=(base + ahead(j), tp), device_id_type=MESH)
     pl.semaphore_signal(barrier, inc=1, device_id=(mirror, tp), device_id_type=MESH)
+    hub = g // 2 + x
+    crossed = (
+        (1, (g + x, g + 1 - x, g + 3 - x)),
+        (2, (hub, g // 2 + 1 - x)),
+        (3, (g // 2 + 1 - x,)),
+    )
+    for at, others in crossed:
+
+        @pl.when(level == at)
+        def _(others=others):
+            for to in others:
+                pl.semaphore_signal(barrier, inc=1, device_id=(to, tp), device_id_type=MESH)
+
     pl.semaphore_signal(barrier, inc=1, device_id=(me, tp_core), device_id_type=MESH)
     pl.semaphore_signal(barrier, inc=1, device_id=(me, tp_y), device_id_type=MESH)
     staged = [
         pltpu.make_async_copy(src, dst, w_sem.at[3 + i])
         for i, (src, dst) in enumerate(
-            ((tokens_in, tokens_ref), (q_in, q_ref), (k_in, k_ref), (v_in, v_ref))
+            (
+                (tokens_in, tokens_ref),
+                (moe_gain_in, moe_gain_ref),
+                (routes_in, routes_ref),
+                (score_in, score_ref),
+                (q_in, q_ref),
+                (k_in, k_ref),
+                (v_in, v_ref),
+                (gain_in, gain_ref),
+                (lam_in, lam_ref),
+            )
         )
     ]
     for c in staged:
@@ -292,7 +326,8 @@
         load.start()
 
     features = pl.ds(pl.multiple_of(tp * width, width), width)
-    staged[0].wait()
+    for c in staged[:3]:
+        c.wait()
     token_f32 = tokens_ref[...].astype(jnp.float32)
     inverse = lax.rsqrt(jnp.mean(token_f32 * token_f32, axis=-1, keepdims=True) + moe_eps)
     dense[...] = (
@@ -332,9 +367,8 @@
         )
 
     choose(0, routes_ref, dense)
-    pl.semaphore_wait(barrier, g + 2)
-
-    for c in staged[1:]:
+    pl.semaphore_wait(barrier, g + 2 + lax.rem(4 - level, 4))
+    for c in staged[3:]:
         c.wait()
     sent = []
     mirrored = [
@@ -361,27 +395,77 @@
             c.start()
             tok_copies[group, j] = c
 
-    unit_copies = {}
-
-    def share(which, src, dst):
-        for j in range(1, g):
-            d = ahead(j)
-            cols = pl.ds(pl.multiple_of(d * VD, VD), VD)
-            c = remote(
-                src.at[:, cols],
-                dst.at[w],
-                a_send.at[which, j],
-                a_recv.at[which, j],
-                base + d,
-                tp,
-            )
-            c.start()
-            unit_copies[which, j] = c
+    def pair(which):
+        return pl.ds(pl.multiple_of(which * 2 * VD, 2 * VD), 2 * VD)
+
+    def unit(which):
+        src, dst = ((k_ref, kk.at[2 + x]), (q_ref, qx.at[x]), (v_ref, vv.at[2 + x]))[which]
+        return remote(
+            src.at[:, pair(1 - x)], dst, a_send.at[which], a_recv.at[which], beside, tp
+        )
+
+    def own_up(which):
+        src, dst = ((k_ref, kk), (v_ref, vv))[which]
+        return remote(
+            src.at[:, pair(x)],
+            dst.at[x],
+            kv_send.at[which, x],
+            kv_recv.at[which, x],
+            me + 2,
+            tp,
+        )
+
+    def other_up(which):
+        buf = (kk, vv)[which]
+        return remote(
+            buf.at[3 - x],
+            buf.at[1 - x],
+            kv_send.at[which, 1 - x],
+            kv_recv.at[which, 1 - x],
+            me + 2,
+            tp,
+        )
+
+    def from_below(which, b):
+        buf = (kk, vv)[which]
+        return remote(
+            buf.at[b], buf.at[b], kv_send.at[which, b], kv_recv.at[which, b], me - 2, tp
+        )
+
+    def own_q():
+        return remote(
+            q_ref.at[:, pair(x)],
+            qm.at[high, x],
+            qm_send.at[high, x],
+            qm_recv.at[high, x],
+            hub,
+            tp,
+        )
+
+    def other_q():
+        return remote(
+            qx.at[1 - x],
+            qm.at[high, 1 - x],
+            qm_send.at[high, 1 - x],
+            qm_recv.at[high, 1 - x],
+            hub,
+            tp,
+        )
+
+    def q_came(late, b):
+        return remote(
+            qm.at[late, b],
+            qm.at[late, b],
+            qm_send.at[late, b],
+            qm_recv.at[late, b],
+            g + 2 * late + x,
+            tp,
+        )
 
     y_copies, core_copies, more_copies = {}, {}, {}
 
     def hand(group, j):
-        s = behind(j)
+        s = ahead(j)
         if j == 0:
             src = tok.at[group, w]
             arr[tp, group, w] = tok[group, w]
@@ -405,31 +489,41 @@
         core_copies[group, j] = c
 
     scatter(0)
-    share(1, q_ref, qb)
+
+    @pl.when(half == 1)
+    def _():
+        unit(1).start()
+
+    unit(0).start()
     hand(0, 0)
-    own = pl.ds(pl.multiple_of(w * VD, VD), VD)
-    kb[w] = k_ref[:, own]
-    qb[w] = q_ref[:, own]
-    vb[w] = v_ref[:, own]
-    for j in range(1, g):
+    kk[2 + x] = k_ref[:, pair(x)]
+    qx[x] = q_ref[:, pair(x)]
+    vv[2 + x] = v_ref[:, pair(x)]
+    for j in (3, 1, 2):
         hand(0, j)
     for c in mirrored:
         c.wait_recv()
     choose(1, routes_m, dense_m)
     scatter(1)
     hand(1, 0)
-    def q_on(s):
-        return remote(qb.at[s], qm.at[s], qm_send.at[s], qm_recv.at[s], mirror, tp)
+    unit(2).start()
+
+    @pl.when(half == 0)
+    def _():
+        unit(1).start()
 
     @pl.when(half == 1)
     def _():
-        for j in range(1, g):
-            unit_copies[1, j].wait_recv()
-        for s in range(g):
-            q_on(s).start()
-
-    share(0, k_ref, kb)
-    share(2, v_ref, vb)
+        own_q().start()
+        unit(1).wait_recv()
+        other_q().start()
+
+    @pl.when(high == 0)
+    def _():
+        own_up(0).start()
+        unit(0).wait_recv()
+        other_up(0).start()
+        own_up(1).start()
 
     def first_products(group, quarter):
         a = arr[quarter, group].reshape(total, width)
@@ -450,8 +544,8 @@
     near_copies, far_copies = {}, {}
 
     def far_half(group, gate, up):
-        for j in range(g):
-            s = behind(j)
+        for j in (0, 3, 1, 2):
+            s = ahead(j)
             y_copies[group, j].wait_recv()
             c = remote(
                 arr.at[tp_y, group, s],
@@ -492,7 +586,7 @@
                 c.start()
                 near_copies[group, h] = c
         near_copies[group, 0].wait_recv()
-        for j in range(g):
+        for j in [*range(1, g), 0]:
             d = ahead(j)
             csum[group, d] = (
                 part[group, 1, d].astype(jnp.float32) + near[group, 0, d].astype(jnp.float32)
@@ -512,7 +606,7 @@
 
     def expert_back(group):
         near_copies[group, 1].wait_recv()
-        for j in range(g):
+        for j in [*range(1, g), 0]:
             d = ahead(j)
             far_copies[group, j].wait_recv()
             val = (
@@ -548,31 +642,27 @@
             combined = combined + raised[c] / (raised[0] + raised[1]) * picked
         return combined
 
-    loads[0].wait()
-    loads[1].wait()
-    gate, up = near_half(0)
-    hidden = far_half(0, gate, up)
-    for j in range(1, g):
-        hand(1, j)
-    loads[2].wait()
-    second_products(0, hidden)
-    lam = lam_ref[w]
+    lam = [lam_ref[x * 2 + h] for h in range(2)]
     size = 2 * rows
-    blocks = g // 2
-    reach = g * rows
     diag = (
         lax.broadcasted_iota(jnp.int32, (size, size), 1)
         <= lax.broadcasted_iota(jnp.int32, (size, size), 0)
     )
     stat_lane = lax.broadcasted_iota(jnp.int32, (size, 128), 1)
 
-    def weigh(q, seen, masked):
+    def columns(h, m):
+        return slice(h * VD + m * QKD, h * VD + (m + 1) * QKD)
+
+    def weigh(q, first, h, masked):
         found = []
+        seen = (4 - first) * rows
         for m in range(2):
-            cols = slice(m * QKD, (m + 1) * QKD)
-            k = kb[0 : seen // rows].reshape(seen, 2 * QKD)[:, cols]
+            k = kk[first:4].reshape(seen, 2 * VD)[:, columns(h, m)]
             scores = lax.dot_general(
-                q[:, cols], k, (((1,), (1,)), ((), ())), preferred_element_type=jnp.float32
+                q[:, columns(h, m)],
+                k,
+                (((1,), (1,)), ((), ())),
+                preferred_element_type=jnp.float32,
             ) * QKD ** (-0.5)
             if masked:
                 last = jnp.where(diag, scores[:, seen - size :], neg_big)
@@ -586,162 +676,252 @@
             found.append((weights, top, jnp.sum(weights, axis=-1, keepdims=True)))
         return found
 
-    def blend(first, second, one, two, seen):
-        v = vb[0 : seen // rows].reshape(seen, VD)
-        mixed = (first * one - second * two).astype(jnp.bfloat16)
+    def blend(one, two, scale_one, scale_two, first, h):
+        v = vv[first:4].reshape((4 - first) * rows, 2 * VD)[:, h * VD : (h + 1) * VD]
+        mixed = (one * scale_one - two * scale_two).astype(jnp.bfloat16)
         return jnp.dot(mixed, v, preferred_element_type=jnp.float32)
 
-    def keep(i, seen, found):
-        (one, top_one, sum_one), (two, top_two, sum_two) = found
-        line = pl.ds(i * size, size)
-        pr[0, line, 0:seen] = one
-        pr[1, line, 0:seen] = two
-        packed = jnp.where(
-            stat_lane == 0,
-            top_one,
-            jnp.where(stat_lane == 1, sum_one, jnp.where(stat_lane == 2, top_two, sum_two)),
-        )
-        stat_out[:, line] = packed.T[0:8]
-
-    def stats_on():
-        return remote(stat_out, stat_in, x_send.at[0], x_recv.at[0], mirror, tp)
-
-    def o_on(i):
-        line = pl.ds(i * size, size)
+    def keep(late, place, q, first, masked):
+        seen = (4 - first) * rows
+        packed = jnp.zeros((size, 128), jnp.float32)
+        for h in range(2):
+            for m, (weights, top, bottom) in enumerate(weigh(q, first, h, masked)):
+                pr[place, h, m, :, 0:seen] = weights
+                packed = jnp.where(stat_lane == 4 * h + 2 * m, top, packed)
+                packed = jnp.where(stat_lane == 4 * h + 2 * m + 1, bottom, packed)
+        stat_out[late] = packed.T[0:8]
+
+    def stats_on(late, to):
         return remote(
-            osend.at[line], oret.at[line], x_send.at[1 + i], x_recv.at[1 + i], mirror, tp
-        )
-
-    def merged():
-        mine, other = stat_out[...], stat_in[...]
-        scale = []
-        for m in range(2):
-            top, bottom = mine[2 * m : 2 * m + 1], mine[2 * m + 1 : 2 * m + 2]
-            top_o, bottom_o = other[2 * m : 2 * m + 1], other[2 * m + 1 : 2 * m + 2]
-            high = jnp.maximum(top, top_o)
-            part_mine = jnp.exp(top - high)
-            scale.append(part_mine / (bottom * part_mine + bottom_o * jnp.exp(top_o - high)))
-        at = lax.broadcasted_iota(jnp.int32, (128, reach), 0)
-        both = jnp.where(at == 0, scale[0], jnp.where(at == 1, scale[1] * lam, 0.0))
-        return both.T
-
-    def f_on(d):
-        return remote(fin.at[d], att_in.at[w], f_send.at[d], f_recv.at[w], base + d, tp)
-
-    def finish(i, mixed):
+            stat_out.at[late], stat_in.at[late], st_send.at[late], st_recv.at[late], to, tp
+        )
+
+    def merged(late):
+        mine, other = stat_out[late], stat_in[late]
+        at = lax.broadcasted_iota(jnp.int32, (128, size), 0)
+        table = jnp.zeros((128, size), jnp.float32)
+        for h in range(2):
+            for m in range(2):
+                r = 4 * h + 2 * m
+                top, bottom = mine[r : r + 1], mine[r + 1 : r + 2]
+                top_o, bottom_o = other[r : r + 1], other[r + 1 : r + 2]
+                high_top = jnp.maximum(top, top_o)
+                share = jnp.exp(top - high_top)
+                scale = share / (bottom * share + bottom_o * jnp.exp(top_o - high_top))
+                if m == 1:
+                    scale = scale * lam[h]
+                table = jnp.where(at == 2 * h + m, scale, table)
+        return table.T
+
+    def o_on(late, h, b):
+        return remote(
+            osend.at[late, h, b],
+            oret.at[x, h],
+            o_send.at[late, h, b],
+            o_recv.at[x, h],
+            g + 2 * late + b,
+            tp,
+        )
+
+    def o_came(side, h):
+        return remote(
+            oret.at[side, h],
+            oret.at[side, h],
+            o_send.at[0, h, 0],
+            o_recv.at[side, h],
+            g // 2 + side,
+            tp,
+        )
+
+    def f_on(h):
+        return remote(fin.at[h, 1 - x], att_in.at[h], f_send.at[h], f_recv.at[h], beside, tp)
+
+    def normal(mixed):
         scaled = mixed * lax.rsqrt(jnp.mean(mixed * mixed, axis=-1, keepdims=True) + head_eps)
-        scaled = (scaled * gain_ref[...] * head_scale).astype(jnp.bfloat16)
-        fin[2 * i : 2 * i + 2] = scaled.reshape(2, rows, VD)
-        for d in (2 * i, 2 * i + 1):
-
-            @pl.when(d != w)
-            def _(d=d):
-                f_on(d).start()
-
-            @pl.when(d == w)
-            def _(d=d):
-                att_in[w] = fin[d]
+        return (scaled * gain_ref[...] * head_scale).astype(jnp.bfloat16)
+
+    def finish(h, mixed):
+        fin[h] = normal(mixed).reshape(2, rows, VD)
+        f_on(h).start()
+
+    def own_rows():
+        return qx[...].reshape(size, 2 * VD)
+
+    def below_came(which):
+        for b in range(2):
+            from_below(which, b).wait_recv()
+
+    def settle(first):
+        for h in range(2):
+            one, two = weigh(own_rows(), first, h, True)
+            finish(h, blend(one[0], two[0], 1.0 / one[2], lam[h] / two[2], first, h))
+
+    def late_scores(late):
+        for b in range(2):
+            q_came(late, b).wait_recv()
+        keep(late, late, qm[late].reshape(size, 2 * VD), 0, False)
+        stats_on(late, g + 2 * late + x).start()
+
+    def late_out(late):
+        stats_on(late, g + 2 * late + x).wait_recv()
+        scales = merged(late)
+        for h in range(2):
+            o = blend(
+                pr[late, h, 0],
+                pr[late, h, 1],
+                scales[:, 2 * h : 2 * h + 1],
+                scales[:, 2 * h + 1 : 2 * h + 2],
+                0,
+                h,
+            )
+            osend[late, h] = o.astype(jnp.bfloat16).reshape(2, rows, VD)
+            for b in range(2):
+                o_on(late, h, b).start()
+
+    def own_late(late, first):
+        seen = (4 - first) * rows
+        stats_on(late, hub).wait_recv()
+        scales = merged(late)
+        for h in range(2):
+            o = blend(
+                pr[0, h, 0, :, 0:seen],
+                pr[0, h, 1, :, 0:seen],
+                scales[:, 2 * h : 2 * h + 1],
+                scales[:, 2 * h + 1 : 2 * h + 2],
+                first,
+                h,
+            ).reshape(2, rows, VD)
+            olate[h] = o
+            fin[h] = o.astype(jnp.bfloat16)
+            f_on(h).start()
+
+    at_level = [level == i for i in range(4)]
+
+    loads[0].wait()
+    loads[1].wait()
+    gate, up = near_half(0)
+    hidden = far_half(0, gate, up)
+    for j in (3, 1, 2):
+        hand(1, j)
+    loads[2].wait()
+    second_products(0, hidden)
+
+    @pl.when(at_level[2])
+    def _():
+        keep(0, 0, own_rows(), 2, True)
+        stats_on(0, hub).start()
+
+    @pl.when(at_level[3])
+    def _():
+        unit(0).wait_recv()
+        below_came(0)
+        keep(1, 0, own_rows(), 0, True)
+        stats_on(1, hub).start()
 
     gate, up = near_half(1)
+
+    @pl.when(high == 0)
+    def _():
+        unit(2).wait_recv()
+        other_up(1).start()
+
+    @pl.when(at_level[1])
+    def _():
+        unit(0).wait_recv()
+        below_came(0)
+        late_scores(0)
+
     hidden = far_half(1, gate, up)
     second_products(1, hidden)
 
-    for j in range(1, g):
-        unit_copies[0, j].wait_recv()
-
-    @pl.when(half == 1)
-    def _():
-        for i in range(blocks):
-            q = qb[2 * i : 2 * i + 2].reshape(size, 2 * QKD)
-            seen = (i + 1) * size
-            keep(i, seen, weigh(q, seen, True))
-        stats_on().start()
-
-    @pl.when(half == 0)
-    def _():
-        for s in range(g):
-            q_on(s).wait_recv()
-        for i in range(blocks):
-            q = qm[2 * i : 2 * i + 2].reshape(size, 2 * QKD)
-            keep(i, reach, weigh(q, reach, False))
-        stats_on().start()
-
-    for j in range(1, g):
-        unit_copies[2, j].wait_recv()
-    stats_on().wait_recv()
-    scales = merged()
-
-    @pl.when(half == 0)
-    def _():
-        for i in range(blocks):
-            line = pl.ds(i * size, size)
-            part_scale = scales[i * size : (i + 1) * size]
-            osend[line] = blend(
-                pr[0, line], pr[1, line], part_scale[:, 0:1], part_scale[:, 1:2], reach
-            ).astype(jnp.bfloat16)
-            o_on(i).start()
+    @pl.when(at_level[1])
+    def _():
+        late_scores(1)
+        unit(2).wait_recv()
+        below_came(1)
+        late_out(0)
+        late_out(1)
 
     expert_back(0)
 
-    @pl.when(half == 0)
-    def _():
-        for j in range(1, g):
-            unit_copies[1, j].wait_recv()
-        for i in range(blocks):
-            q = qb[2 * i : 2 * i + 2].reshape(size, 2 * QKD)
-            seen = (i + 1) * size
-            one, two = weigh(q, seen, True)
-            finish(i, blend(one[0], two[0], 1.0 / one[2], lam / two[2], seen))
+    @pl.when(at_level[0])
+    def _():
+        unit(1).wait_recv()
+        settle(2)
+
+    @pl.when(at_level[2])
+    def _():
+        own_late(0, 2)
+
+    @pl.when(at_level[3])
+    def _():
+        unit(2).wait_recv()
+        below_came(1)
+        own_late(1, 0)
 
     expert_back(1)
+
+    @pl.when(at_level[1])
+    def _():
+        unit(1).wait_recv()
+        settle(0)
+
     back[...] = combine(1, score_m).astype(jnp.bfloat16)
     last = remote(back, back_m, m_send.at[3], m_recv.at[3], mirror, tp)
     last.start()
     sent.append(last)
+    combined = combine(0, score_ref)
+
+    def head_columns(side, h):
+        return pl.ds(pl.multiple_of((2 * side + h) * VD, VD), VD)
 
     @pl.when(half == 1)
     def _():
-        for i in range(blocks):
-            line = pl.ds(i * size, size)
-            seen = (i + 1) * size
-            part_scale = scales[i * size : (i + 1) * size]
-            mixed = blend(
-                pr[0, line, 0:seen],
-                pr[1, line, 0:seen],
-                part_scale[:, 0:1],
-                part_scale[:, 1:2],
-                seen,
+        for h in range(2):
+            o_came(x, h).wait_recv()
+            att_ref[:, head_columns(x, h)] = normal(
+                olate[h, x] + oret[x, h].astype(jnp.float32)
             )
-            o_on(i).wait_recv()
-            finish(i, mixed + oret[line].astype(jnp.float32))
-
-    combined = combine(0, score_ref)
-
-    for h in range(heads):
-
-        @pl.when(h != w)
-        def _(h=h):
-            remote(fin.at[h], att_in.at[h], f_send.at[h], f_recv.at[h], base + h, tp).wait()
-
-        att_ref[:, h * VD : (h + 1) * VD] = att_in[h]
+        for h in range(2):
+            f_on(h).wait()
+            o_came(1 - x, h).wait_recv()
+            att_ref[:, head_columns(1 - x, h)] = normal(
+                att_in[h].astype(jnp.float32) + oret[1 - x, h].astype(jnp.float32)
+            )
+
+    @pl.when(half == 0)
+    def _():
+        for h in range(2):
+            att_ref[:, head_columns(x, h)] = fin[h, x]
+        for h in range(2):
+            f_on(h).wait()
+            att_ref[:, head_columns(1 - x, h)] = att_in[h]
 
     last.wait_recv()
     out_ref[...] = (combined + back_m[...].astype(jnp.float32)).astype(jnp.bfloat16)
 
     @pl.when(half == 1)
     def _():
-        for s in range(g):
-            q_on(s).wait_send()
-
-    @pl.when(half == 0)
-    def _():
-        for i in range(blocks):
-            o_on(i).wait_send()
-
-    stats_on().wait_send()
+        own_q().wait_send()
+        other_q().wait_send()
+        stats_on(high, hub).wait_send()
+
+    @pl.when(high == 0)
+    def _():
+        for which in range(2):
+            own_up(which).wait_send()
+            other_up(which).wait_send()
+
+    @pl.when(at_level[1])
+    def _():
+        for late in range(2):
+            stats_on(late, g + 2 * late + x).wait_send()
+            for h in range(2):
+                for b in range(2):
+                    o_on(late, h, b).wait_send()
+
     for group in (
         tok_copies,
-        unit_copies,
         y_copies,
         core_copies,
         more_copies,
@@ -752,6 +932,8 @@
         sent += list(group.values())
     for c in sent:
         c.wait_send()
+    for which in range(3):
+        unit(which).wait_send()
 
 
 def local(
@@ -777,7 +959,6 @@
     ff = w_gate.shape[2]
     vmem = pl.BlockSpec(memory_space=pltpu.VMEM)
     hbm = pl.BlockSpec(memory_space=pl.ANY)
-    smem = pl.BlockSpec(memory_space=pltpu.SMEM)
     bf16, f32 = jnp.bfloat16, jnp.float32
     g = n // 2
     dma = pltpu.SemaphoreType.DMA
@@ -789,23 +970,24 @@
     held = pl.pallas_call(
         functools.partial(step_kernel, n, heads),
         out_shape=inside,
-        in_specs=[hbm, hbm, hbm, smem, vmem, hbm] + [vmem] * 3 + [hbm, hbm, hbm],
+        in_specs=[hbm] * 12,
         out_specs=(vmem, vmem),
         scratch_shapes=[
             pltpu.VMEM((model, ff), bf16),
             pltpu.VMEM((model, ff), bf16),
             pltpu.VMEM((ff, model), bf16),
-            pltpu.VMEM((g, rows, VD), bf16),
-            pltpu.VMEM((g, rows, VD), bf16),
-            pltpu.VMEM((g, rows, VD), bf16),
-            pltpu.VMEM((g, rows, VD), bf16),
-            pltpu.VMEM((2, g * rows, g * rows), f32),
-            pltpu.VMEM((8, g * rows), f32),
-            pltpu.VMEM((8, g * rows), f32),
-            pltpu.VMEM((g * rows, VD), bf16),
-            pltpu.VMEM((g * rows, VD), bf16),
-            pltpu.VMEM((g, rows, VD), bf16),
-            pltpu.VMEM((heads, rows, VD), bf16),
+            pltpu.VMEM((2, rows, 2 * VD), bf16),
+            pltpu.VMEM((4, rows, 2 * VD), bf16),
+            pltpu.VMEM((4, rows, 2 * VD), bf16),
+            pltpu.VMEM((2, 2, rows, 2 * VD), bf16),
+            pltpu.VMEM((2, 2, 2, 2 * rows, 4 * rows), f32),
+            pltpu.VMEM((2, 8, 2 * rows), f32),
+            pltpu.VMEM((2, 8, 2 * rows), f32),
+            pltpu.VMEM((2, 2, 2, rows, VD), bf16),
+            pltpu.VMEM((2, 2, rows, VD), bf16),
+            pltpu.VMEM((2, 2, rows, VD), f32),
+            pltpu.VMEM((2, 2, rows, VD), bf16),
+            pltpu.VMEM((2, rows, VD), bf16),
             pltpu.VMEM((TOP, rows_b), jnp.int32),
             pltpu.VMEM((TOP, rows_b), f32),
             pltpu.VMEM((rows_b, width), bf16),
@@ -825,7 +1007,12 @@
             pltpu.VMEM(queries.shape, bf16),
             pltpu.VMEM(queries.shape, bf16),
             pltpu.VMEM(tokens.shape, bf16),
-            dma((7,)),
+            pltpu.SMEM(lambdas.shape, f32),
+            pltpu.VMEM((1, VD), f32),
+            pltpu.VMEM((1, model), f32),
+            pltpu.VMEM((TOP, rows_b), jnp.int32),
+            pltpu.VMEM((TOP, rows_b), f32),
+            dma((12,)),
             dma((4,)),
             dma((4,)),
             dma((2, g)),
@@ -834,14 +1021,18 @@
             dma((2, g)),
             dma((2, 2, g)),
             dma((2, 2, g)),
-            dma((3, g)),
-            dma((3, g)),
-            dma((g,)),
-            dma((g,)),
-            dma((1 + g // 2,)),
-            dma((1 + g // 2,)),
-            dma((g,)),
-            dma((g,)),
+            dma((3,)),
+            dma((3,)),
+            dma((2, 2)),
+            dma((2, 2)),
+            dma((2, 2)),
+            dma((2, 2)),
+            dma((2,)),
+            dma((2,)),
+            dma((2, 2, 2)),
+            dma((2, 2)),
+            dma((2,)),
+            dma((2,)),
             dma((2, 2)),
             dma((2, 2)),
             dma((2, g)),
@@ -871,7 +1062,7 @@
 
 def fits(mesh, head_count):
     n, parts = mesh.shape["ep"], mesh.shape["tp"]
-    return parts == 4 and n % 2 == 0 and 2 * (head_count // parts) == n
+    return parts == 4 and n == 2 * parts and head_count == parts * parts
 
 
 def solution(mesh):

time: 55.8 us -> 52.6 us (0.943)
  the two profiles are of different devices: /device:TPU:26 before, /device:TPU:0 now
where the time goes in v2:
time: 52.6 us; the launch traced here: 52.5 us
  Pallas kernels  50.5 us (96%)
  local copies, waits for them, and re-layouts  1.36 us (3%)
  between operations  0.64 us (1%)
    pallas_call x1, Pallas kernels, local(): pl.pallas_call(functools.partial(step_kernel, n, heads), out_shape=inside...  50.5 us
    unnamed x2, local copies, waits for them, and re-layouts  1.36 us

profile of v2, /device:TPU:0, one launch (start us, length us, event | category | flops | bytes accessed | tf_op | source)
XLA Modules:
  0.0 52.5 jit_solution(10327619797842598945)
XLA Ops:
  0.6 50.5 %shard_map.131 = (bf16[128,1024]{1,0:T(8,128)(2,1)S(1)}, bf16[64,1024]{1,0:T(8,128)(2,1)S(1)}) custom-call(bf16[128,1024]{1,0:T(8,128)(2,1)} %q_in.1, bf16[128,1024]{1,0:T(8,128)(2,1)} %k_in.1, bf16[128,1024]{1,0:T(8,128)(2,1)} %v_in.1, f32[4]{0:T(128)} %lam_in.1, f32[1,256]{1,0:T(1,128)} %bitcast.5, bf16[64,4096]{1,0:T(8,128)(2,1)} %tokens_in.1, ...), custom_call_target="tpu_custom_call" | custom-call | tf_op jit(solution)/shard_map/pallas_call | solution.py:970
  51.1 0.7 %copy.16 = bf16[128,1024]{1,0:T(8,128)(2,1)} copy(bf16[128,1024]{1,0:T(8,128)(2,1)S(1)} %get-tuple-element.2) | data formatting | bytes 524288
  51.8 0.7 %copy.17 = bf16[64,1024]{1,0:T(8,128)(2,1)} copy(bf16[64,1024]{1,0:T(8,128)(2,1)S(1)} %get-tuple-element.3) | data formatting | bytes 262144

commit v3 on v2

--- a/solution.py
+++ b/solution.py
@@ -586,60 +586,67 @@
                 c.start()
                 near_copies[group, h] = c
         near_copies[group, 0].wait_recv()
+        for c in range(2):
+            cols = pl.ds(c * width // 2, width // 2)
+            for j in [*range(1, g), 0]:
+                d = ahead(j)
+                csum[group, d, :, cols] = (
+                    part[group, 1, d, :, cols].astype(jnp.float32)
+                    + near[group, 0, d, :, cols].astype(jnp.float32)
+                ).astype(jnp.bfloat16)
+                far_copies[group, c, j] = remote(
+                    csum.at[group, d, :, cols],
+                    far.at[group, d, :, cols],
+                    ry_send.at[group, c, j],
+                    ry_recv.at[group, c, j],
+                    me,
+                    tp_y,
+                )
+                far_copies[group, c, j].start()
+
+    back_copies = {}
+
+    def expert_back(group, c):
+        if c == 0:
+            near_copies[group, 1].wait_recv()
+        cols = pl.ds(c * width // 2, width // 2)
         for j in [*range(1, g), 0]:
             d = ahead(j)
-            csum[group, d] = (
-                part[group, 1, d].astype(jnp.float32) + near[group, 0, d].astype(jnp.float32)
-            ).astype(jnp.bfloat16)
-            c = remote(
-                csum.at[group, d],
-                far.at[group, d],
-                ry_send.at[group, j],
-                ry_recv.at[group, j],
-                me,
-                tp_y,
-            )
-            c.start()
-            far_copies[group, j] = c
-
-    back_copies = {}
-
-    def expert_back(group):
-        near_copies[group, 1].wait_recv()
-        for j in [*range(1, g), 0]:
-            d = ahead(j)
-            far_copies[group, j].wait_recv()
+            far_copies[group, c, j].wait_recv()
             val = (
-                part[group, 3, d].astype(jnp.float32)
-                + near[group, 1, d].astype(jnp.float32)
-                + far[group, d].astype(jnp.float32)
+                part[group, 3, d, :, cols].astype(jnp.float32)
+                + near[group, 1, d, :, cols].astype(jnp.float32)
+                + far[group, d, :, cols].astype(jnp.float32)
             ).astype(jnp.bfloat16)
             if j == 0:
-                ret[group, w] = val
+                ret[group, w, :, cols] = val
             else:
-                res[group, d] = val
-                c = remote(
-                    res.at[group, d],
-                    ret.at[group, w],
-                    e_send.at[group, j],
-                    e_recv.at[group, j],
+                res[group, d, :, cols] = val
+                back_copies[group, c, j] = remote(
+                    res.at[group, d, :, cols],
+                    ret.at[group, w, :, cols],
+                    e_send.at[group, c, j],
+                    e_recv.at[group, c, j],
                     base + d,
                     tp,
                 )
-                c.start()
-                back_copies[group, j] = c
-
-    def combine(group, ref):
-        for j in range(1, g):
-            back_copies[group, j].wait_recv()
+                back_copies[group, c, j].start()
+
+    def shares_of(ref):
         first, second = upright(ref, 0), upright(ref, 1)
         top = jnp.maximum(first, second)
         raised = (jnp.exp(first - top), jnp.exp(second - top))
-        returned = ret[group].reshape(total, width)
-        combined = jnp.zeros(out_ref.shape, jnp.float32)
-        for c in range(TOP):
-            picked = jnp.dot(pick[group, c], returned, preferred_element_type=jnp.float32)
-            combined = combined + raised[c] / (raised[0] + raised[1]) * picked
+        return [raised[k] / (raised[0] + raised[1]) for k in range(TOP)]
+
+    def combine(group, c, gates):
+        for j in range(1, g):
+            back_copies[group, c, j].wait_recv()
+        cols = pl.ds(c * width // 2, width // 2)
+        returned = ret[group, :, :, cols].reshape(total, width // 2)
+        combined = jnp.zeros((rows_b, width // 2), jnp.float32)
+        for k in range(TOP):
+            picked = jnp.dot(pick[group, k], returned, preferred_element_type=jnp.float32)
+            combined = combined + gates[k] * picked
         return combined
 
     lam = [lam_ref[x * 2 + h] for h in range(2)]
@@ -825,24 +832,22 @@
         unit(2).wait_recv()
         other_up(1).start()
 
+    hidden = far_half(1, gate, up)
+    second_products(1, hidden)
+
     @pl.when(at_level[1])
     def _():
         unit(0).wait_recv()
         below_came(0)
         late_scores(0)
-
-    hidden = far_half(1, gate, up)
-    second_products(1, hidden)
-
-    @pl.when(at_level[1])
-    def _():
         late_scores(1)
         unit(2).wait_recv()
         below_came(1)
         late_out(0)
         late_out(1)
 
-    expert_back(0)
+    expert_back(0, 0)
+    expert_back(0, 1)
 
     @pl.when(at_level[0])
     def _():
@@ -859,18 +864,32 @@
         below_came(1)
         own_late(1, 0)
 
-    expert_back(1)
+    expert_back(1, 0)
+    expert_back(1, 1)
 
     @pl.when(at_level[1])
     def _():
         unit(1).wait_recv()
         settle(0)
 
-    back[...] = combine(1, score_m).astype(jnp.bfloat16)
-    last = remote(back, back_m, m_send.at[3], m_recv.at[3], mirror, tp)
-    last.start()
-    sent.append(last)
-    combined = combine(0, score_ref)
+    gates = shares_of(score_m)
+    lasts = []
+    for c in range(2):
+        cols = pl.ds(c * width // 2, width // 2)
+        back[:, cols] = combine(1, c, gates).astype(jnp.bfloat16)
+        last = remote(
+            back.at[:, cols],
+            back_m.at[:, cols],
+            m_send.at[3 + c],
+            m_recv.at[3 + c],
+            mirror,
+            tp,
+        )
+        last.start()
+        lasts.append(last)
+    sent += lasts
+    gates = shares_of(score_ref)
+    combined = [combine(0, c, gates) for c in range(2)]
 
     def head_columns(side, h):
         return pl.ds(pl.multiple_of((2 * side + h) * VD, VD), VD)
@@ -897,8 +916,12 @@
             f_on(h).wait()
             att_ref[:, head_columns(1 - x, h)] = att_in[h]
 
-    last.wait_recv()
-    out_ref[...] = (combined + back_m[...].astype(jnp.float32)).astype(jnp.bfloat16)
+    for c in range(2):
+        cols = pl.ds(c * width // 2, width // 2)
+        lasts[c].wait_recv()
+        out_ref[:, cols] = (combined[c] + back_m[:, cols].astype(jnp.float32)).astype(
+            jnp.bfloat16
+        )
 
     @pl.when(half == 1)
     def _():
@@ -1013,8 +1036,8 @@
             pltpu.VMEM((TOP, rows_b), jnp.int32),
             pltpu.VMEM((TOP, rows_b), f32),
             dma((12,)),
-            dma((4,)),
-            dma((4,)),
+            dma((5,)),
+            dma((5,)),
             dma((2, g)),
             dma((2, g)),
             dma((2, g)),
@@ -1035,10 +1058,10 @@
             dma((2,)),
             dma((2, 2)),
             dma((2, 2)),
-            dma((2, g)),
-            dma((2, g)),
-            dma((2, g)),
-            dma((2, g)),
+            dma((2, 2, g)),
+            dma((2, 2, g)),
+            dma((2, 2, g)),
+            dma((2, 2, g)),
         ],
         compiler_params=pltpu.CompilerParams(
             collective_id=0, has_side_effects=True, vmem_limit_bytes=56 * 1024 * 1024

time: 52.6 us -> 51.6 us (0.981)
  Pallas kernels: 50.5 us -> 49.4 us
    pallas_call x1, Pallas kernels: 50.5 us -> 49.4 us  [local(): pl.pallas_call(functools.partial(step_kernel, n, heads), out_shape=inside...]
where the time goes in v3:
time: 51.6 us; the launch traced here: 51.4 us
  Pallas kernels  49.4 us (96%)
  local copies, waits for them, and re-layouts  1.36 us (3%)
  between operations  0.64 us (1%)
    pallas_call x1, Pallas kernels, local(): pl.pallas_call(functools.partial(step_kernel, n, heads), out_shape=inside...  49.4 us
    unnamed x2, local copies, waits for them, and re-layouts  1.36 us

profile of v3, /device:TPU:0, one launch (start us, length us, event | category | flops | bytes accessed | tf_op | source)
XLA Modules:
  0.0 51.4 jit_solution(13517687449211022411)
XLA Ops:
  0.6 49.4 %shard_map.131 = (bf16[128,1024]{1,0:T(8,128)(2,1)S(1)}, bf16[64,1024]{1,0:T(8,128)(2,1)S(1)}) custom-call(bf16[128,1024]{1,0:T(8,128)(2,1)} %q_in.1, bf16[128,1024]{1,0:T(8,128)(2,1)} %k_in.1, bf16[128,1024]{1,0:T(8,128)(2,1)} %v_in.1, f32[4]{0:T(128)} %lam_in.1, f32[1,256]{1,0:T(1,128)} %bitcast.5, bf16[64,4096]{1,0:T(8,128)(2,1)} %tokens_in.1, ...), custom_call_target="tpu_custom_call" | custom-call | tf_op jit(solution)/shard_map/pallas_call | solution.py:993
  50.1 0.7 %copy.16 = bf16[128,1024]{1,0:T(8,128)(2,1)} copy(bf16[128,1024]{1,0:T(8,128)(2,1)S(1)} %get-tuple-element.2) | data formatting | bytes 524288
  50.8 0.7 %copy.17 = bf16[64,1024]{1,0:T(8,128)(2,1)} copy(bf16[64,1024]{1,0:T(8,128)(2,1)S(1)} %get-tuple-element.3) | data formatting | bytes 262144
